TPU v7x, 256 devices: a whole 4x4x8 slice. The times are simulated.
256 devices in a mesh: kv: 32 (over z, y), tp: 8 (over x, core).
Axes of the slice: x: 4, y: 4, z: 8, core: 2. Of those that a mesh axis runs over, the one named last changes fastest.
Arguments:
- tokens: bfloat16 [128, 4096], P(None, 'kv'), may hold values from -8 to 8, as said below
- attn_gain: float32 [4096], P('kv'), may hold values from 0.1 to 1.9
- query_weight: bfloat16 [4096, 1024], P('kv', 'tp'), may hold values from -0.09375 to 0.09375
- key_weight: bfloat16 [4096, 1024], P('kv', 'tp'), may hold values from -0.09375 to 0.09375
- value_weight: bfloat16 [4096, 2048], P('kv', 'tp'), may hold values from -0.09375 to 0.09375
- outgate_weight: bfloat16 [4096, 2048], P('kv', 'tp'), may hold values from -0.09375 to 0.09375
- code_weight: bfloat16 [4096, 16], P('kv'), may hold values from -0.09375 to 0.09375
- decay_weight: bfloat16 [16, 1024], P(None, 'tp'), may hold values from -6 to 6
- decay_bias: float32 [1024], P('tp'), may hold values from -4 to 2
- head_gain: float32 [256], replicated, may hold values from 0.1 to 1.9
- key_cache: bfloat16 [128, 64, 8, 128], P('kv', None, 'tp'), may hold values from -6 to 6
- value_cache: bfloat16 [128, 64, 8, 256], P('kv', None, 'tp'), may hold values from -6 to 6
- decay_cache: float32 [128, 64, 8, 128], P('kv', None, 'tp'), may hold values from -1.1 to 0
- carried_state: float32 [128, 8, 128, 256], P('kv', 'tp'), may hold values from -24 to 24
- lengths: int32 [128], P('kv'), may hold values from 1 to 64, 3328 in all
- output_weight: bfloat16 [2048, 4096], P('tp', 'kv'), may hold values from -0.125 to 0.125
- mlp_gain: float32 [4096], P('kv'), may hold values from 0.1 to 1.9
- gate_weight: bfloat16 [4096, 11008], P('kv', 'tp'), may hold values from -0.09375 to 0.09375
- up_weight: bfloat16 [4096, 11008], P('kv', 'tp'), may hold values from -0.09375 to 0.09375
- down_weight: bfloat16 [11008, 4096], P('tp', 'kv'), may hold values from -0.0546875 to 0.0546875
Outputs:
- layer_out: bfloat16 [128, 4096], P(None, 'kv')
- new_keys: bfloat16 [128, 8, 128], P('kv', 'tp')
- new_values: bfloat16 [128, 8, 256], P('kv', 'tp')
Inputs may be any that keep to these rules, and one draw needn't show every extreme that they name: `tokens`: the features of a row have unlike scales. Sequence b's new token comes right after its lengths[b] live positions; positions from lengths[b] on take no part.
All inputs are finite; a program needn't handle non-finite values. No bound on the sum of `lengths` on one device may be relied on, other than what follows from the above.
Results may differ from a plain program's by a relative error of at most 0.025.
Values may be sent and summed in bfloat16 or wider, within the bound.
A program may use at most 64 MiB of HBM per device.

v0:
```python
import jax
import jax.numpy as jnp
from jax import lax
from jax.sharding import PartitionSpec as P

WIDTH = 4096


EPS = 1e-06
GATE_TEMP = 16.0


def sent_to_all(x, axis):
    length = lax.axis_size(axis)
    return lax.all_to_all(jnp.broadcast_to(x[None], (length, *x.shape)), axis, 0, 0, tiled=True)


def taken_together(x, axis):
    everything = sent_to_all(x, axis)
    return jnp.sum(everything.astype(jnp.float32), axis=0)


def split_up(x, dim, length):
    dims = x.shape
    tiles = x.reshape(*dims[:dim], length, dims[dim] // length, *dims[dim + 1 :])
    return jnp.moveaxis(tiles, dim, 0)


def sent_and_summed(x, axis, dim):
    length = lax.axis_size(axis)
    tiles = lax.all_to_all(split_up(x, dim, length), axis, 0, 0, tiled=True)
    return jnp.sum(tiles.astype(jnp.float32), axis=0)


def side_by_side(arrays, axis, dim, along):
    columns = [a.reshape(*a.shape[:along], -1) for a in arrays]
    both = jnp.concatenate(columns, axis=along)
    out, at, done = (sent_and_summed(both, axis, dim), 0, [])
    for a, column in zip(arrays, columns):
        share = out[..., at : at + column.shape[along]]
        done.append(share.reshape(*share.shape[:along], *a.shape[along:]))
        at += column.shape[along]
    return tuple(done)


def joined_along(tiles, dim):
    tiles = jnp.moveaxis(tiles, 0, dim)
    dims = tiles.shape
    return tiles.reshape(*dims[:dim], dims[dim] * dims[dim + 1], *dims[dim + 2 :])


def gathered_copies(x, axis, dim):
    tiles = sent_to_all(x, axis)
    return joined_along(tiles, dim)


def across_heads(partial_value):
    return taken_together(partial_value.astype(jnp.bfloat16), "tp").astype(jnp.float32)


def block_attention(
    queries,
    new_keys,
    new_values,
    new_decay,
    key_cache,
    value_cache,
    decay_cache,
    carried_state,
    lengths,
):
    positions = jnp.arange(key_cache.shape[1], dtype=jnp.int32)
    live_mask = positions[None, :] < lengths[:, None]
    kept_decay = jnp.where(live_mask[:, :, None, None], decay_cache, jnp.zeros_like(decay_cache))
    later_sum = lax.cumsum(kept_decay, axis=1, reverse=True) - kept_decay
    total_decay = jnp.sum(kept_decay, axis=1)
    decayed = queries.astype(jnp.float32) * jnp.exp(new_decay)
    carried = jnp.einsum("bhd,bhde->bhe", decayed * jnp.exp(total_decay), carried_state)
    keyed_cache = key_cache.astype(jnp.float32) * jnp.exp(later_sum)
    scores = jnp.einsum("bhd,bshd->bhs", decayed, keyed_cache)
    scores = jnp.where(live_mask[:, None, :], scores, jnp.zeros_like(scores)).astype(jnp.bfloat16)
    within = jnp.einsum("bhs,bshe->bhe", scores, value_cache, preferred_element_type=jnp.float32)
    own_score = jnp.sum(queries.astype(jnp.float32) * new_keys.astype(jnp.float32), axis=-1)
    return carried + within + own_score[..., None] * new_values.astype(jnp.float32)


def mixer_hidden(gate_sum, up_sum, square_sum):
    inv_mid = lax.rsqrt(square_sum / WIDTH + EPS)[:, None]
    return (jax.nn.silu(gate_sum * inv_mid) * (up_sum * inv_mid)).astype(jnp.bfloat16)


def on_device(
    tokens,
    attn_gain,
    query_weight,
    key_weight,
    value_weight,
    outgate_weight,
    code_weight,
    decay_weight,
    decay_bias,
    head_gain,
    key_cache,
    value_cache,
    decay_cache,
    carried_state,
    lengths,
    output_weight,
    mlp_gain,
    gate_weight,
    up_weight,
    down_weight,
):
    local_seqs, heads_here, key_dim, value_dim = carried_state.shape
    token_f = tokens.astype(jnp.float32)
    scaled = (token_f * attn_gain[None, :]).astype(jnp.bfloat16)
    query_part = jnp.dot(scaled, query_weight, preferred_element_type=jnp.float32)
    key_part = jnp.dot(scaled, key_weight, preferred_element_type=jnp.float32)
    value_part = jnp.dot(scaled, value_weight, preferred_element_type=jnp.float32)
    outgate_part = jnp.dot(scaled, outgate_weight, preferred_element_type=jnp.float32)
    code_part = jnp.dot(scaled, code_weight, preferred_element_type=jnp.float32)
    token_squares = jnp.sum(token_f * token_f, axis=1)
    query_sum, key_sum, value_sum, outgate_sum, code_sum, square_sum = side_by_side(
        (
            query_part.astype(jnp.bfloat16),
            key_part.astype(jnp.bfloat16),
            value_part.astype(jnp.bfloat16),
            outgate_part.astype(jnp.bfloat16),
            code_part.astype(jnp.bfloat16),
            token_squares.astype(jnp.bfloat16),
        ),
        "kv",
        0,
        1,
    )
    inv_rms = lax.rsqrt(square_sum / WIDTH + EPS)[:, None]
    queries = (
        (query_sum * inv_rms * key_dim ** (-0.5))
        .astype(jnp.bfloat16)
        .reshape(local_seqs, heads_here, key_dim)
    )
    new_keys = (key_sum * inv_rms).astype(jnp.bfloat16).reshape(local_seqs, heads_here, key_dim)
    new_values = (
        (value_sum * inv_rms).astype(jnp.bfloat16).reshape(local_seqs, heads_here, value_dim)
    )
    out_gate = (
        (outgate_sum * inv_rms).astype(jnp.bfloat16).reshape(local_seqs, heads_here, value_dim)
    )
    gate_code = (code_sum * inv_rms).astype(jnp.bfloat16)
    pre_gate = (
        jnp.dot(gate_code, decay_weight, preferred_element_type=jnp.float32) + decay_bias[None, :]
    )
    new_decay = (jax.nn.log_sigmoid(pre_gate) / GATE_TEMP).reshape(local_seqs, heads_here, key_dim)
    mixed_heads = block_attention(
        queries,
        new_keys,
        new_values,
        new_decay,
        key_cache,
        value_cache,
        decay_cache,
        carried_state,
        lengths,
    )
    normed = (
        mixed_heads
        * lax.rsqrt(jnp.mean(mixed_heads * mixed_heads, axis=-1, keepdims=True) + EPS)
        * head_gain
    )
    heads_out = (
        (normed * jax.nn.silu(out_gate.astype(jnp.float32)))
        .astype(jnp.bfloat16)
        .reshape(local_seqs, heads_here * value_dim)
    )
    attended = across_heads(
        jnp.dot(
            gathered_copies(heads_out, "kv", 0), output_weight, preferred_element_type=jnp.float32
        )
    )
    middle = (token_f + attended).astype(jnp.bfloat16)
    mid_f = middle.astype(jnp.float32)
    scaled_mid = (mid_f * mlp_gain[None, :]).astype(jnp.bfloat16)
    gate_part = jnp.dot(scaled_mid, gate_weight, preferred_element_type=jnp.float32)
    up_part = jnp.dot(scaled_mid, up_weight, preferred_element_type=jnp.float32)
    mid_squares = jnp.sum(mid_f * mid_f, axis=1)
    gate_sum, up_sum, mid_sum = side_by_side(
        (
            gate_part.astype(jnp.bfloat16),
            up_part.astype(jnp.bfloat16),
            mid_squares.astype(jnp.bfloat16),
        ),
        "kv",
        0,
        1,
    )
    hidden_share = mixer_hidden(gate_sum, up_sum, mid_sum)
    lifted_part = jnp.dot(
        gathered_copies(hidden_share, "kv", 0), down_weight, preferred_element_type=jnp.float32
    )
    layer_out = (mid_f + across_heads(lifted_part)).astype(jnp.bfloat16)
    return (layer_out, new_keys, new_values)


def solution(mesh):
    in_specs = (
        P(None, "kv"),
        P("kv"),
        P("kv", "tp"),
        P("kv", "tp"),
        P("kv", "tp"),
        P("kv", "tp"),
        P("kv", None),
        P(None, "tp"),
        P("tp"),
        P(),
        P("kv", None, "tp", None),
        P("kv", None, "tp", None),
        P("kv", None, "tp", None),
        P("kv", "tp", None, None),
        P("kv"),
        P("tp", "kv"),
        P("kv"),
        P("kv", "tp"),
        P("kv", "tp"),
        P("tp", "kv"),
    )
    out_specs = (P(None, "kv"), P("kv", "tp", None), P("kv", "tp", None))
    return jax.shard_map(
        on_device, mesh=mesh, in_specs=in_specs, out_specs=out_specs, check_vma=False
    )
```

profile of v0, /device:TPU:1, one launch (start us, length us, event | category | flops | bytes accessed | tf_op | source)
XLA Modules:
  0.0 119.1 jit_solution(6003303624993991082)
XLA Ops:
  0.6 0.9 fusion.7
  1.6 0.9 convolution_convert_fusion.8
  2.6 0.2 convert_element_type.167
  2.9 0.9 convolution_convert_fusion.7
  3.8 0.9 convolution_convert_fusion.6
  4.7 1.0 convolution_convert_fusion.3
  5.8 1.1 convolution_convert_fusion.2
  6.9 0.9 concatenate.27
  7.9 12.0 %all-to-all-start = ((bf16[32,4,785]{2,1,0:T(4,128)(2,1)}), bf16[32,4,785]{2,1,0:T(4,128)(2,1)S(1)}, u32[]{:S(2)}, u32[]{:S(2)}) async-start(bf16[32,4,785]{2,1,0:T(4,128)(2,1)} %concatenate.27), calls=%async_computation | async-start | bytes 458752 | tf_op jit(solution)/shard_map/all_to_all | solution.py:31
  20.0 1.9 %fusion.22 = (f32[4,128]{1,0:T(4,128)S(1)}, f32[4,64,1,128]{3,2,1,0:T(1,128)S(1)}) fusion(f32[4,64,1,128]{3,2,1,0:T(1,128)S(1)} %copy-done.2, pred[4,64]{1,0:T(4,128)(4,1)S(1)} %iota_compare_fusion, bf16[4,64,1,128]{3,1,2,0:T(8,128)(2,1)S(1)} %copy-done.7), kind=kOutput, calls=%fused_computation.40 | output fusion | flops 2260480 | bytes 329984 | tf_op jit(solution)/shard_map/block_attention/reduce_window_sum | solution.py:75
  21.9 8.8 %all-to-all-done = bf16[32,4,785]{2,1,0:T(4,128)(2,1)S(1)} async-done(((bf16[32,4,785]{2,1,0:T(4,128)(2,1)}), bf16[32,4,785]{2,1,0:T(4,128)(2,1)S(1)}, u32[]{:S(2)}, u32[]{:S(2)}) %all-to-all-start) | async-done | bytes 200992 | tf_op jit(solution)/shard_map/all_to_all | solution.py:31
  30.9 0.2 fusion.41
  31.0 0.8 fusion.30
  31.8 0.2 exponential_multiply_fusion
  32.5 0.2 multiply_reduce_fusion
  32.7 0.7 fusion.49
  33.4 13.2 %all_to_all.30 = bf16[32,4,256]{2,1,0:T(4,128)(2,1)S(1)} all-to-all(bf16[32,4,256]{2,1,0:T(4,128)(2,1)S(1)} %broadcast_in_dim.23), channel_id=1, replica_groups=mesh['kv'=32,'tp'=8] {'kv'}, dimensions={0} | all-to-all | bytes 131072 | tf_op jit(solution)/shard_map/all_to_all | solution.py:15
  46.9 13.3 %all_to_all.31 = bf16[8,128,128]{2,1,0:T(8,128)(2,1)S(1)} all-to-all(bf16[8,128,128]{2,1,0:T(8,128)(2,1)S(1)} %broadcast_in_dim.24), channel_id=1, replica_groups=mesh['kv'=32,'tp'=8] {'tp'}, dimensions={0} | all-to-all | bytes 524288 | tf_op jit(solution)/shard_map/all_to_all | solution.py:15
  60.4 0.2 convert_element_type.168
  60.6 0.3 convolution_convert_fusion
  60.9 0.2 copy.36
  61.2 0.7 copy-done.4
  61.9 0.3 convolution_convert_fusion.1
  62.1 0.2 copy.35
  62.4 1.9 %concatenate.30 = bf16[32,4,2753]{2,1,0:T(4,128)(2,1)S(1)} concatenate(bf16[32,4,1376]{2,1,0:T(4,128)(2,1)S(1)} %concatenate.28, bf16[32,4,1376]{2,1,0:T(4,128)(2,1)S(1)} %concatenate.29, bf16[32,4,1]{2,1,0:T(4,128)(2,1)S(1)} %convert_element_type.168), dimensions={2} | concatenate | bytes 1409536 | tf_op jit(solution)/shard_map/concatenate | solution.py:37
  64.3 23.0 %all_to_all.32 = bf16[32,4,2753]{2,1,0:T(4,128)(2,1)S(1)} all-to-all(bf16[32,4,2753]{2,1,0:T(4,128)(2,1)S(1)} %concatenate.30), channel_id=1, replica_groups=mesh['kv'=32,'tp'=8] {'kv'}, dimensions={0} | all-to-all | bytes 1409536 | tf_op jit(solution)/shard_map/all_to_all | solution.py:31
  87.3 0.3 convert_reduce_fusion
  87.6 0.2 fusion.36
  88.0 16.9 %all_to_all.33 = bf16[32,4,1376]{2,1,0:T(4,128)(2,1)S(1)} all-to-all(bf16[32,4,1376]{2,1,0:T(4,128)(2,1)S(1)} %broadcast_in_dim.25), channel_id=1, replica_groups=mesh['kv'=32,'tp'=8] {'kv'}, dimensions={0} | all-to-all | bytes 704512 | tf_op jit(solution)/shard_map/all_to_all | solution.py:15
  105.1 0.3 convolution_convert_fusion.4
  105.4 13.0 %all_to_all.34 = bf16[8,128,128]{2,1,0:T(8,128)(2,1)S(1)} all-to-all(bf16[8,128,128]{2,1,0:T(8,128)(2,1)S(1)} %broadcast_in_dim.26), channel_id=1, replica_groups=mesh['kv'=32,'tp'=8] {'tp'}, dimensions={0} | all-to-all | bytes 524288 | tf_op jit(solution)/shard_map/all_to_all | solution.py:15
  118.5 0.6 fusion.11
  (50 shorter events, 2.0 us)
Async XLA Ops:
  0.6 31.6 %copy-start = (f32[4,1,128,256]{3,2,1,0:T(8,128)S(1)}, f32[4,1,128,256]{3,2,1,0:T(8,128)}, u32[]{:S(2)}) copy-start(f32[4,1,128,256]{3,2,1,0:T(8,128)} %param.33) | copy-start | bytes 1572868
  5.8 14.1 %copy-start.11 = (s32[4]{0:T(128)S(1)}, s32[4]{0:T(128)}, u32[]{:S(2)}) copy-start(s32[4]{0:T(128)} %param.34) | copy-start | bytes 52
  5.8 14.2 %copy-start.2 = (f32[4,64,1,128]{3,2,1,0:T(1,128)S(1)}, f32[4,64,1,128]{3,2,1,0:T(1,128)}, u32[]{:S(2)}) copy-start(f32[4,64,1,128]{3,2,1,0:T(1,128)} %param.32) | copy-start | bytes 393220
  5.8 14.2 %copy-start.7 = (bf16[4,64,1,128]{3,1,2,0:T(8,128)(2,1)S(1)}, bf16[4,64,1,128]{3,1,2,0:T(8,128)(2,1)}, u32[]{:S(2)}) copy-start(bf16[4,64,1,128]{3,1,2,0:T(8,128)(2,1)} %param.30) | copy-start | bytes 196612
  6.9 24.9 %copy-start.12 = (bf16[16,128]{1,0:T(8,128)(2,1)S(1)}, bf16[16,128]{1,0:T(8,128)(2,1)}, u32[]{:S(2)}) copy-start(bf16[16,128]{1,0:T(8,128)(2,1)} %param.27) | copy-start | bytes 12292
  6.9 24.9 %copy-start.13 = (f32[128]{0:T(128)S(1)}, f32[128]{0:T(128)}, u32[]{:S(2)}) copy-start(f32[128]{0:T(128)} %param.28) | copy-start | bytes 1540
  7.9 22.9 %all-to-all-start = ((bf16[32,4,785]{2,1,0:T(4,128)(2,1)}), bf16[32,4,785]{2,1,0:T(4,128)(2,1)S(1)}, u32[]{:S(2)}, u32[]{:S(2)}) async-start(bf16[32,4,785]{2,1,0:T(4,128)(2,1)} %concatenate.27), calls=%async_computation | async-start | bytes 458752 | tf_op jit(solution)/shard_map/all_to_all | solution.py:31
  20.0 12.4 %copy-start.6 = (bf16[4,64,1,256]{3,1,2,0:T(8,128)(2,1)S(1)}, bf16[4,64,1,256]{3,1,2,0:T(8,128)(2,1)}, u32[]{:S(2)}) copy-start(bf16[4,64,1,256]{3,1,2,0:T(8,128)(2,1)} %param.31) | copy-start | bytes 393220
  20.0 12.8 %copy-start.10 = (f32[256]{0:T(256)S(1)}, f32[256]{0:T(256)}, u32[]{:S(2)}) copy-start(f32[256]{0:T(256)} %param.29) | copy-start | bytes 3076
  21.9 24.7 %copy-start.8 = (bf16[256,128]{1,0:T(8,128)(2,1)S(1)}, bf16[256,128]{1,0:T(8,128)(2,1)}, u32[]{:S(2)}) copy-start(bf16[256,128]{1,0:T(8,128)(2,1)} %param.35) | copy-start | bytes 196612
  46.6 13.6 %copy-start.1 = (bf16[128,128]{1,0:T(8,128)(2,1)S(1)}, bf16[128,128]{1,0:T(8,128)(2,1)}, u32[]{:S(2)}) copy-start(bf16[128,128]{1,0:T(8,128)(2,1)} %param.20) | copy-start | bytes 98308
  46.7 14.0 %copy-start.3 = (bf16[128,1376]{0,1:T(8,128)(2,1)S(1)}, bf16[128,1376]{0,1:T(8,128)(2,1)}, u32[]{:S(2)}) copy-start(bf16[128,1376]{0,1:T(8,128)(2,1)} %param.38) | copy-start | bytes 1056772
  46.7 14.0 %copy-start.9 = (f32[128]{0:T(128)S(1)}, f32[128]{0:T(128)}, u32[]{:S(2)}) copy-start(f32[128]{0:T(128)} %param.36) | copy-start | bytes 1540
  60.9 1.0 copy-start.4
  88.0 17.1 %copy-start.5 = (bf16[1376,128]{1,0:T(8,128)(2,1)S(1)}, bf16[1376,128]{1,0:T(8,128)(2,1)}, u32[]{:S(2)}) copy-start(bf16[1376,128]{1,0:T(8,128)(2,1)} %param.39) | copy-start | bytes 1056772
where the time goes:
time: 120 us; the launch traced here: 119 us
  blocking collectives  79.5 us (66%)
  starting transfers between devices  12 us (10%)
  waiting for transfers between devices  8.83 us (7%)
  matrix products  6.39 us (5%)
  other arithmetic  6.27 us (5%)
  local copies, waits for them, and re-layouts  5.17 us (4%)
    all_to_all x4, blocking collectives, sent_to_all(): lax.all_to_all(jnp.broadcast_to(x[None], (length, *x.shape)), axis, 0, 0,...  56.5 us
    all_to_all x1, blocking collectives, sent_and_summed(): tiles = lax.all_to_all(split_up(x, dim, length), axis, 0, 0, tiled=True)  23 us
    all_to_all x1, starting transfers between devices, sent_and_summed(): tiles = lax.all_to_all(split_up(x, dim, length), axis, 0, 0, tiled=True)  12 us
    all_to_all x1, waiting for transfers between devices, sent_and_summed(): tiles = lax.all_to_all(split_up(x, dim, length), axis, 0, 0, tiled=True)  8.83 us
    concatenate x6, local copies, waits for them, and re-layouts, side_by_side(): both = jnp.concatenate(columns, axis=along)  3.03 us
  transfers between devices with their start and end apart: 1, of which 1 were waited for; matrix products, arithmetic and copies ran while one was open for 2% of the time, Pallas kernels for 0%

commit v1 on v0

v1 whole, which is shorter than its diff:
```python
import functools

import jax
import jax.numpy as jnp
from jax import lax
from jax.experimental import pallas as pl
from jax.experimental.pallas import tpu as pltpu
from jax.sharding import PartitionSpec as P

MESH = pl.DeviceIdType.MESH
F32 = jnp.float32
BF16 = jnp.bfloat16
EPS = 1e-06
GATE_TEMP = 16.0
NY = 4
UNIT = 16


def dot(a, b):
    return jnp.dot(a, b, preferred_element_type=F32)


def dot_nt(a, b):
    return lax.dot_general(a, b, (((1,), (1,)), ((), ())), preferred_element_type=F32)


class Plan:
    def __init__(self, n_kv, n_tp, rows, feat, kd, vd, rank, hid, span):
        self.kv, self.tp, self.rows, self.feat = n_kv, n_tp, rows, feat
        self.kd, self.vd, self.rank, self.hid, self.span = kd, vd, rank, hid, span
        self.nz = n_kv // NY
        self.seqs = rows // n_kv
        self.width = feat * n_kv
        self.cols = 2 * kd + 2 * vd + 128
        units = -(-hid // (UNIT * NY))
        self.per_y = units * UNIT
        self.cnt = [UNIT * (units // self.nz + (1 if z < units % self.nz else 0)) for z in range(self.nz)]
        self.off = [sum(self.cnt[:z]) for z in range(self.nz)]
        self.pr = max(self.cnt)
        half = self.nz // 2
        step = max(1, half // 2)
        self.a_subs = [list(range(i, i + step)) for i in range(0, half, step)]
        self.b_subs = [list(range(i, i + step)) for i in range(half, self.nz, step)]
        self.subs = self.a_subs + self.b_subs
        self.na = len(self.a_subs)
        self.has_sq = [i in (0, self.na) for i in range(len(self.subs))]
        self.sub_rows = [
            (UNIT if sq else 0) + sum(2 * self.cnt[z] for z in zs)
            for sq, zs in zip(self.has_sq, self.subs)
        ]
        self.piece = UNIT + 2 * self.pr


def kernel(pn, *refs):
    it = iter(refs)
    take = lambda n: [next(it) for _ in range(n)]
    (
        tok_h, again_h, wq_h, wk_h, wv_h, wg_h, wc_h, dwt_h, bias_h, hgain_h,
        kc_h, vc_h, dc_h, st_h, len_h, ow_h, mgain_h, gw_h, uw_h, dn_h,
    ) = take(20)
    out_ref, nk_ref, nv_ref = take(3)
    (
        tok, again, wq, wk, wv, wg, wc, dwt, bias, hgain, kc, vc, dc, st, lens, ow, mgain, gw, uw, dn,
    ) = take(20)
    (f1, p1, r1, keyed, etot, stb, owt, tokt, mgt, dnp, dnt, g1, g1f, x1, midt, x2, spc, zin, hb) = take(19)
    ns = len(pn.subs)
    psub = take(ns)
    rin = take(ns)
    qin = take(ns)
    cin = take(ns)
    cout = take(ns)
    (
        in_sem, s1s, s1r, g1s, g1r, x1s, x1r, x2s, x2r,
        rss, rsr, qss, qsr, css, csr, zss, zsr, hzs, hzr, hls, hlr, hrs, hrr, hfs, hfr,
    ) = take(25)

    kv = lax.axis_index("kv")
    tp = lax.axis_index("tp")
    nz, n_kv, n_tp = pn.nz, pn.kv, pn.tp
    y = lax.rem(kv, NY)
    z = kv // NY
    yr, yl, yo = lax.rem(y + 1, NY), lax.rem(y + 3, NY), lax.rem(y + 2, NY)
    right, left = z * NY + yr, z * NY + yl

    pairs = [
        (tok_h, tok), (again_h, again), (wq_h, wq), (wk_h, wk), (wv_h, wv), (wg_h, wg),
        (wc_h, wc.at[pl.ds(0, pn.rank)]),
        (dc_h, dc), (len_h, lens), (kc_h, kc), (st_h, st), (dwt_h, dwt.at[pl.ds(0, pn.rank)]),
        (bias_h, bias), (hgain_h, hgain), (vc_h, vc), (ow_h, ow), (mgain_h, mgain),
    ]
    last = pn.hid - (NY - 1) * pn.per_y
    for src, dst in ((gw_h, gw), (uw_h, uw), (dn_h, dn)):
        for i in range(NY):
            size = pn.per_y if i < NY - 1 else last
            pairs.append((src.at[pl.ds(i * pn.per_y, size)], dst.at[i, pl.ds(0, size)]))
    wc[...] = jnp.zeros_like(wc)
    dwt[...] = jnp.zeros_like(dwt)
    loads = [pltpu.make_async_copy(s, d, in_sem.at[i]) for i, (s, d) in enumerate(pairs)]
    for c in loads:
        c.start()

    barrier = pltpu.get_barrier_semaphore()

    @pl.loop(1, n_kv)
    def _(d):
        pl.semaphore_signal(barrier, inc=1, device_id={"kv": lax.rem(kv + d, n_kv)}, device_id_type=MESH)

    @pl.loop(1, n_tp)
    def _(d):
        pl.semaphore_signal(barrier, inc=1, device_id={"tp": lax.rem(tp + d, n_tp)}, device_id_type=MESH)

    def remote(src, dst, ssem, rsem, **where):
        return pltpu.make_async_remote_copy(
            src_ref=src, dst_ref=dst, send_sem=ssem, recv_sem=rsem, device_id=where, device_id_type=MESH
        )

    def drain(ref, sem):
        pltpu.make_async_copy(ref, ref, sem).wait()

    for c in loads[:7]:
        c.wait()
    tok_f = tok[...].astype(F32)
    scaled = (tok_f * again[...]).astype(BF16)
    kd, vd = pn.kd, pn.vd
    f1[:, 0:kd] = dot(scaled, wq[...])
    f1[:, kd : 2 * kd] = dot(scaled, wk[...])
    f1[:, 2 * kd : 2 * kd + vd] = dot(scaled, wv[...])
    f1[:, 2 * kd + vd : 2 * kd + 2 * vd] = dot(scaled, wg[...])
    code = dot_nt(scaled, wc[...])
    squares = jnp.sum(tok_f * tok_f, axis=1, keepdims=True)
    lane = lax.broadcasted_iota(jnp.int32, code.shape, 1)
    f1[:, 2 * kd + 2 * vd :] = jnp.where(lane == pn.rank, squares, code)
    for p in range(n_kv):
        p1[p] = f1[p * pn.seqs : (p + 1) * pn.seqs, :].astype(BF16)
    pl.semaphore_wait(barrier, n_kv + n_tp - 2)

    @pl.loop(1, n_kv)
    def _(d):
        peer = lax.rem(kv + d, n_kv)
        remote(p1.at[peer], r1.at[kv], s1s, s1r, kv=peer).start()

    r1[kv] = p1[kv]

    for c in loads[7:17]:
        c.wait()
    pos = lax.broadcasted_iota(jnp.int32, (pn.span, kd), 0)
    for b in range(pn.seqs):
        live = pos < lens[b]
        kept = jnp.where(live, dc[b], 0.0)
        run = kept
        shift = 1
        while shift < pn.span:
            moved = pltpu.roll(run, pn.span - shift, 0)
            run = run + jnp.where(pos < pn.span - shift, moved, 0.0)
            shift *= 2
        keyed[b] = jnp.where(live, kc[b].astype(F32) * jnp.exp(run - kept), 0.0)
        etot[b : b + 1, :] = jnp.exp(run[0:1, :])
        stb[b] = st[b].astype(BF16)
    tokt[...] = tok_f.T
    mgt[...] = jnp.broadcast_to(mgain[...], (pn.rows, pn.feat)).T
    for i in range(vd // 128):
        owt[:, i * 128 : (i + 1) * 128] = ow[i * 128 : (i + 1) * 128, :].astype(F32).T.astype(BF16)
    for c in loads[17:]:
        c.wait()
    pad = NY * pn.per_y - pn.hid
    if pad:
        for ref in (gw, uw, dn):
            ref[NY - 1, pn.per_y - pad :, :] = jnp.zeros((pad, pn.feat), BF16)
    dnp[...] = jnp.zeros_like(dnp)
    spc[...] = jnp.zeros_like(spc)
    for i in range(NY):
        for zz in range(nz):
            dnp[i, zz * pn.pr : zz * pn.pr + pn.cnt[zz], :] = dn[i, pn.off[zz] : pn.off[zz] + pn.cnt[zz], :]
        for j in range(nz * pn.pr // 128):
            dnt[i, :, j * 128 : (j + 1) * 128] = (
                dnp[i, j * 128 : (j + 1) * 128, :].astype(F32).T.astype(BF16)
            )

    drain(r1.at[pl.ds(0, n_kv - 1)], s1r)
    sums = jnp.zeros((pn.seqs, pn.cols), F32)
    for p in range(n_kv):
        sums = sums + r1[p].astype(F32)
    tail = sums[:, 2 * kd + 2 * vd :]
    inv = lax.rsqrt(tail[:, pn.rank : pn.rank + 1] / pn.width + EPS)
    queries = (sums[:, 0:kd] * inv * kd ** (-0.5)).astype(BF16).astype(F32)
    new_keys = (sums[:, kd : 2 * kd] * inv).astype(BF16)
    new_values = (sums[:, 2 * kd : 2 * kd + vd] * inv).astype(BF16)
    out_gate = (sums[:, 2 * kd + vd : 2 * kd + 2 * vd] * inv).astype(BF16).astype(F32)
    nk_ref[...] = new_keys
    nv_ref[...] = new_values
    pre = dot((tail * inv).astype(BF16), dwt[...]) + bias[...]
    new_decay = (jnp.minimum(pre, 0.0) - jnp.log1p(jnp.exp(-jnp.abs(pre)))) / GATE_TEMP
    decayed = queries * jnp.exp(new_decay)
    faded = (decayed * etot[...]).astype(BF16)
    own = jnp.sum(queries * new_keys.astype(F32), axis=1, keepdims=True)
    rows = []
    for b in range(pn.seqs):
        scores = jnp.sum(decayed[b : b + 1, :] * keyed[b], axis=1, keepdims=True).astype(BF16).astype(F32)
        within = jnp.sum(scores * vc[b].astype(F32), axis=0, keepdims=True)
        rows.append(dot(faded, stb[b])[b : b + 1, :] + within)
    mixed = jnp.concatenate(rows, axis=0) + own * new_values.astype(F32)
    normed = mixed * lax.rsqrt(jnp.mean(mixed * mixed, axis=1, keepdims=True) + EPS) * hgain[...]
    heads = normed * (out_gate / (1.0 + jnp.exp(-out_gate)))
    g1[kv] = heads.astype(BF16)

    @pl.loop(1, n_kv)
    def _(d):
        peer = lax.rem(kv + d, n_kv)
        remote(g1.at[kv], g1.at[kv], g1s, g1r, kv=peer).start()

    drain(g1.at[pl.ds(0, n_kv - 1)], g1r)
    for p in range(n_kv):
        g1f[p * pn.seqs : (p + 1) * pn.seqs, :] = g1[p].astype(F32)

    def summed_over_tp(part, buf, ssem, rsem):
        buf[tp] = part.astype(BF16)

        @pl.loop(1, n_tp)
        def _(d):
            peer = lax.rem(tp + d, n_tp)
            remote(buf.at[tp], buf.at[tp], ssem, rsem, tp=peer).start()

        drain(buf.at[pl.ds(0, n_tp - 1)], rsem)
        total = buf[0].astype(F32)
        for i in range(1, n_tp):
            total = total + buf[i].astype(F32)
        return total

    attended = summed_over_tp(dot_nt(owt[...], g1f[...].astype(BF16)), x1, x1s, x1r)
    mid = (tokt[...] + attended).astype(BF16)
    mid_f = mid.astype(F32)
    midt[...] = mid_f
    scaled_mid = (mid_f * mgt[...]).astype(BF16)
    sq_rows = jnp.broadcast_to(jnp.sum(mid_f * mid_f, axis=0, keepdims=True), (UNIT, pn.rows)).astype(BF16)

    def fill(dest):
        gate = dot(gw[dest], scaled_mid).astype(BF16)
        up = dot(uw[dest], scaled_mid).astype(BF16)
        for s, zs in enumerate(pn.subs):
            at = 0
            if pn.has_sq[s]:
                psub[s][dest, 0:UNIT, :] = sq_rows
                at = UNIT
            for zz in zs:
                o, n = pn.off[zz], pn.cnt[zz]
                psub[s][dest, at : at + n, :] = gate[o : o + n, :]
                psub[s][dest, at + n : at + 2 * n, :] = up[o : o + n, :]
                at += 2 * n

    def toward(s):
        return right if s < pn.na else left

    def against(s):
        return left if s < pn.na else right

    fill(yo)
    for s in range(ns):
        remote(psub[s].at[yo], rin[s], rss.at[s], rsr.at[s], kv=toward(s)).start()
    fill(yr)
    for s in range(pn.na, ns):
        remote(psub[s].at[yr], qin[s], qss.at[s], qsr.at[s], kv=right).start()
    fill(yl)
    for s in range(pn.na):
        remote(psub[s].at[yl], qin[s], qss.at[s], qsr.at[s], kv=left).start()
    fill(y)
    order = []
    for i in range(max(pn.na, ns - pn.na)):
        order += [s for s in (i, pn.na + i) if (s < pn.na) == (s == i)]
    for s in order:
        nxt = yr if s < pn.na else yl
        drain(rin[s], rsr.at[s])
        cout[s][...] = (psub[s][nxt].astype(F32) + rin[s][...].astype(F32)).astype(BF16)
        remote(cout[s], cin[s], css.at[s], csr.at[s], kv=toward(s)).start()
    sq_sum = {}
    for s in order:
        drain(qin[s], qsr.at[s])
        drain(cin[s], csr.at[s])
        total = (psub[s][y].astype(F32) + qin[s][...].astype(F32) + cin[s][...].astype(F32)).astype(BF16)
        side = s < pn.na
        at = 0
        if pn.has_sq[s]:
            sq_sum[side] = total[0:UNIT, :]
            at = UNIT
        for zz in pn.subs[s]:
            n = pn.cnt[zz]
            spc[zz, 0:UNIT, :] = sq_sum[side]
            spc[zz, UNIT : UNIT + n, :] = total[at : at + n, :]
            spc[zz, UNIT + pn.pr : UNIT + pn.pr + n, :] = total[at + n : at + 2 * n, :]
            at += 2 * n

            @pl.when(z != zz)
            def _(zz=zz):
                remote(spc.at[zz], zin.at[z], zss, zsr, kv=zz * NY + y).start()

    zin[z] = spc[z]
    drain(zin.at[pl.ds(0, nz - 1)], zsr)
    total = zin[0].astype(F32)
    for i in range(1, nz):
        total = total + zin[i].astype(F32)
    inv_mid = lax.rsqrt(total[0:1, :] / pn.width + EPS)
    gate = total[UNIT : UNIT + pn.pr, :] * inv_mid
    up = total[UNIT + pn.pr :, :] * inv_mid
    hb[y, z] = (gate / (1.0 + jnp.exp(-gate)) * up).astype(BF16)

    for d in range(1, nz):
        remote(hb.at[y, z], hb.at[y, z], hzs.at[d], hzr.at[d], kv=lax.rem(z + d, nz) * NY + y).start()

    def slot(d):
        return lax.rem(z + nz - d, nz)

    def spread(d):
        if d:
            drain(hb.at[y, slot(d)], hzr.at[d])
        mine = hb.at[y, slot(d)]
        remote(mine, mine, hls.at[d], hlr.at[d], kv=right).start()
        remote(mine, mine, hrs.at[d], hrr.at[d], kv=left).start()

    def forward(d):
        drain(hb.at[yl, slot(d)], hlr.at[d])
        drain(hb.at[yr, slot(d)], hrr.at[d])
        if d % 2 == 0:
            other = hb.at[yl, slot(d)]
            remote(other, other, hfs.at[d], hfr.at[d], kv=right).start()
        else:
            other = hb.at[yr, slot(d)]
            remote(other, other, hfs.at[d], hfr.at[d], kv=left).start()

    near = sorted(range(nz), key=lambda d: min(d, nz - d))
    head, rest = near[:3], near[3:]
    for d in head:
        spread(d)
    forward(near[0])
    for d in rest:
        spread(d)
    for d in near[1:]:
        forward(d)

    def lifted_from(row):
        return dot(dnt[row], hb[row].reshape(nz * pn.pr, pn.rows))

    lifted = lifted_from(y) + lifted_from(yl) + lifted_from(yr)
    for d in near:
        drain(hb.at[yo, slot(d)], hfr.at[d])
    lifted = lifted + lifted_from(yo)
    final = midt[...] + summed_over_tp(lifted, x2, x2s, x2r)
    out_ref[...] = final.T.astype(BF16)

    drain(p1.at[pl.ds(0, n_kv - 1)], s1s)
    drain(g1.at[pl.ds(0, n_kv - 1)], g1s)
    drain(x1.at[pl.ds(0, n_tp - 1)], x1s)
    drain(x2.at[pl.ds(0, n_tp - 1)], x2s)
    for s in range(ns):
        drain(rin[s], rss.at[s])
        drain(qin[s], qss.at[s])
        drain(cin[s], css.at[s])
    drain(zin.at[pl.ds(0, nz - 1)], zss)
    for d in range(nz):
        if d:
            drain(hb.at[0, 0], hzs.at[d])
        drain(hb.at[0, 0], hls.at[d])
        drain(hb.at[0, 0], hrs.at[d])
        drain(hb.at[0, 0], hfs.at[d])


def on_device(n_kv, n_tp, *args):
    (
        tokens, attn_gain, query_weight, key_weight, value_weight, outgate_weight, code_weight,
        decay_weight, decay_bias, head_gain, key_cache, value_cache, decay_cache, carried_state,
        lengths, output_weight, mlp_gain, gate_weight, up_weight, down_weight,
    ) = args
    rows, feat = tokens.shape
    seqs, span, _, kd = key_cache.shape
    vd = value_cache.shape[-1]
    rank = code_weight.shape[1]
    hid = gate_weight.shape[1]
    pn = Plan(n_kv, n_tp, rows, feat, kd, vd, rank, hid, span)
    operands = (
        tokens, attn_gain.reshape(1, feat), query_weight, key_weight, value_weight, outgate_weight,
        code_weight.T, decay_weight, decay_bias.reshape(1, kd), head_gain.reshape(1, vd),
        key_cache.reshape(seqs, span, kd), value_cache.reshape(seqs, span, vd),
        decay_cache.reshape(seqs, span, kd), carried_state.reshape(seqs, kd, vd), lengths,
        output_weight, mlp_gain.reshape(1, feat), gate_weight.T, up_weight.T, down_weight,
    )
    nz, pr = pn.nz, pn.pr
    vm = pltpu.VMEM
    dma = pltpu.SemaphoreType.DMA
    ns = len(pn.subs)
    landing = [
        vm((rows, feat), BF16), vm((1, feat), F32), vm((feat, kd), BF16), vm((feat, kd), BF16),
        vm((feat, vd), BF16), vm((feat, vd), BF16), vm((128, feat), BF16), vm((128, kd), BF16),
        vm((1, kd), F32), vm((1, vd), F32), vm((seqs, span, kd), BF16), vm((seqs, span, vd), BF16),
        vm((seqs, span, kd), F32), vm((seqs, kd, vd), F32), pltpu.SMEM((seqs,), jnp.int32),
        vm((vd, feat), BF16), vm((1, feat), F32), vm((NY, pn.per_y, feat), BF16),
        vm((NY, pn.per_y, feat), BF16), vm((NY, pn.per_y, feat), BF16),
    ]
    work = [
        vm((rows, pn.cols), F32), vm((n_kv, seqs, pn.cols), BF16), vm((n_kv, seqs, pn.cols), BF16),
        vm((seqs, span, kd), F32), vm((seqs, kd), F32), vm((seqs, kd, vd), BF16),
        vm((feat, vd), BF16), vm((feat, rows), F32), vm((feat, rows), F32),
        vm((NY, nz * pr, feat), BF16), vm((NY, feat, nz * pr), BF16),
        vm((n_kv, seqs, vd), BF16), vm((rows, vd), F32), vm((n_tp, feat, rows), BF16),
        vm((feat, rows), F32), vm((n_tp, feat, rows), BF16),
        vm((nz, pn.piece, rows), BF16), vm((nz, pn.piece, rows), BF16), vm((NY, nz, pr, rows), BF16),
    ]
    subs = [vm((NY, n, rows), BF16) for n in pn.sub_rows]
    for _ in range(4):
        subs += [vm((n, rows), BF16) for n in pn.sub_rows]
    sems = [dma((17 + 3 * NY,))] + [dma(())] * 8 + [dma((ns,))] * 6 + [dma(())] * 2 + [dma((nz,))] * 8
    out, nk, nv = pl.pallas_call(
        functools.partial(kernel, pn),
        out_shape=(
            jax.ShapeDtypeStruct((rows, feat), BF16),
            jax.ShapeDtypeStruct((seqs, kd), BF16),
            jax.ShapeDtypeStruct((seqs, vd), BF16),
        ),
        in_specs=[pl.BlockSpec(memory_space=pl.ANY)] * len(operands),
        out_specs=(pl.BlockSpec(memory_space=pltpu.VMEM),) * 3,
        scratch_shapes=landing + work + subs + sems,
        compiler_params=pltpu.CompilerParams(
            collective_id=0, has_side_effects=True, vmem_limit_bytes=60 * 1024 * 1024
        ),
        name="decode_step",
    )(*operands)
    return out, nk.reshape(seqs, 1, kd), nv.reshape(seqs, 1, vd)


def solution(mesh):
    in_specs = (
        P(None, "kv"), P("kv"), P("kv", "tp"), P("kv", "tp"), P("kv", "tp"), P("kv", "tp"),
        P("kv", None), P(None, "tp"), P("tp"), P(), P("kv", None, "tp", None),
        P("kv", None, "tp", None), P("kv", None, "tp", None), P("kv", "tp", None, None), P("kv"),
        P("tp", "kv"), P("kv"), P("kv", "tp"), P("kv", "tp"), P("tp", "kv"),
    )
    out_specs = (P(None, "kv"), P("kv", "tp", None), P("kv", "tp", None))
    return jax.shard_map(
        functools.partial(on_device, mesh.shape["kv"], mesh.shape["tp"]),
        mesh=mesh, in_specs=in_specs, out_specs=out_specs, check_vma=False,
    )
```

time: 120 us -> 69.3 us (0.58)
  blocking collectives: 79.5 us -> 0 us
  Pallas kernels: 0 us -> 65.8 us
  starting transfers between devices: 12 us -> 0 us
  waiting for transfers between devices: 8.83 us -> 0 us
  matrix products: 6.39 us -> 0 us
  other arithmetic: 6.27 us -> 0 us
  local copies, waits for them, and re-layouts: 5.17 us -> 2.62 us
    all_to_all x5 -> x0, blocking collectives: 79.5 us -> none  [the longest x4 56.5 us: sent_to_all(): lax.all_to_all(jnp.broadcast_to(x[None], (length, *x.shape)), axis, 0, 0,...]
    pallas_call x0 -> x1, Pallas kernels: none -> 65.8 us  [on_device(): pl.pallas_call(functools.partial(kernel, pn), out_shape=(jax.ShapeDtypeSt...]
    all_to_all x1 -> x0, starting transfers between devices: 12 us -> none  [sent_and_summed(): tiles = lax.all_to_all(split_up(x, dim, length), axis, 0, 0, tiled=True)]
    all_to_all x1 -> x0, waiting for transfers between devices: 8.83 us -> none  [sent_and_summed(): tiles = lax.all_to_all(split_up(x, dim, length), axis, 0, 0, tiled=True)]
    dot_general x13 -> x0, matrix products: 6.39 us -> none  [the longest x1 1.06 us: on_device(): jnp.dot(scaled, outgate_weight, preferred_element_type=jnp.float32)]
    concatenate x6 -> x0, local copies, waits for them, and re-layouts: 3.03 us -> none  [side_by_side(): both = jnp.concatenate(columns, axis=along)]
    reduce_sum x8 -> x0, other arithmetic: 2.46 us -> none  [the longest x1 0.92 us: on_device(): token_squares = jnp.sum(token_f * token_f, axis=1)]
    another operation x1 -> x0, other arithmetic: 1.9 us -> none  [block_attention(): later_sum = lax.cumsum(kept_decay, axis=1, reverse=True) - kept_decay]
  transfers between devices with their start and end apart: 1 -> 0, of which waited for: 1 -> 0; matrix products, arithmetic and copies ran while one was open for 2% -> 0% of each run, Pallas kernels for 0% -> 0%
where the time goes in v1:
time: 69.3 us; the launch traced here: 69.1 us
  Pallas kernels  65.8 us (95%)
  local copies, waits for them, and re-layouts  2.62 us (4%)
    pallas_call x1, Pallas kernels, on_device(): pl.pallas_call(functools.partial(kernel, pn), out_shape=(jax.ShapeDtypeSt...  65.8 us
    unnamed x7, local copies, waits for them, and re-layouts  2.62 us

profile of v1, /device:TPU:1, one launch (start us, length us, event | category | flops | bytes accessed | tf_op | source)
XLA Modules:
  0.0 69.1 jit_solution(1725458074084874290)
XLA Ops:
  0.6 65.8 %decode_step.1 = (bf16[128,128]{1,0:T(8,128)(2,1)}, bf16[4,128]{1,0:T(4,128)(2,1)}, bf16[4,256]{1,0:T(4,128)(2,1)}) custom-call(bf16[128,128]{1,0:T(8,128)(2,1)} %refs_0_.1, f32[1,128]{1,0:T(1,128)} %bitcast.23, bf16[128,128]{1,0:T(8,128)(2,1)} %refs_2_.1, bf16[128,128]{1,0:T(8,128)(2,1)} %refs_3_.1, bf16[128,256]{1,0:T(8,128)(2,1)} %refs_4_.1, ...), custom_call_target="tpu_custom_call" | custom-call | tf_op jit(solution)/shard_map/decode_step/pallas_call | solution.py:409
  66.4 0.0 copy-start.1
  66.4 1.4 %copy.26 = bf16[128,128]{1,0:T(8,128)(2,1)} copy(bf16[128,128]{1,0:T(8,128)(2,1)} %get-tuple-element.12) | data formatting | bytes 65536
  67.8 0.0 copy-done.1
  67.8 0.0 copy-start
  67.8 0.6 copy.27
  68.4 0.1 copy-done
  68.5 0.6 copy.28
Async XLA Ops:
  66.4 1.4 %copy-start.1 = (bf16[4,128]{1,0:T(4,128)(2,1)S(1)}, bf16[4,128]{1,0:T(4,128)(2,1)}, u32[]{:S(2)}) copy-start(bf16[4,128]{1,0:T(4,128)(2,1)} %get-tuple-element.7) | copy-start | bytes 3076
  67.8 0.7 copy-start

commit v2 on v1

--- a/solution.py
+++ b/solution.py
@@ -43,12 +43,16 @@
         self.b_subs = [list(range(i, i + step)) for i in range(half, self.nz, step)]
         self.subs = self.a_subs + self.b_subs
         self.na = len(self.a_subs)
-        self.has_sq = [i in (0, self.na) for i in range(len(self.subs))]
-        self.sub_rows = [
-            (UNIT if sq else 0) + sum(2 * self.cnt[z] for z in zs)
-            for sq, zs in zip(self.has_sq, self.subs)
-        ]
-        self.piece = UNIT + 2 * self.pr
+        self.sub_rows = [sum(2 * self.cnt[z] for z in zs) for zs in self.subs]
+        ring = lambda d, n: min(d, n - d)
+        self.kv_far = sorted(
+            [(dz, dy) for dz in range(self.nz) for dy in range(NY) if dz or dy],
+            key=lambda o: -ring(o[0], self.nz) - ring(o[1], NY),
+        )
+        nx = n_tp // 2
+        self.tp_far = sorted(
+            [(dx, dc) for dx in range(nx) for dc in range(2) if dx or dc], key=lambda o: -2 * ring(o[0], nx) - o[1]
+        )
 
 
 def kernel(pn, *refs):
@@ -62,7 +66,7 @@
     (
         tok, again, wq, wk, wv, wg, wc, dwt, bias, hgain, kc, vc, dc, st, lens, ow, mgain, gw, uw, dn,
     ) = take(20)
-    (f1, p1, r1, keyed, etot, stb, owt, tokt, mgt, dnp, dnt, g1, g1f, x1, midt, x2, spc, zin, hb) = take(19)
+    (f1, p1, r1, keyed, etot, stb, owt, tokt, mgt, dnp, dnt, g1, g1f, x1, midt, x2, spc, zin, hb, sqb) = take(20)
     ns = len(pn.subs)
     psub = take(ns)
     rin = take(ns)
@@ -71,8 +75,8 @@
     cout = take(ns)
     (
         in_sem, s1s, s1r, g1s, g1r, x1s, x1r, x2s, x2r,
-        rss, rsr, qss, qsr, css, csr, zss, zsr, hzs, hzr, hls, hlr, hrs, hrr, hfs, hfr,
-    ) = take(25)
+        sqs, sqr, rss, rsr, qss, qsr, css, csr, zss, zsr, hzs, hzr, hls, hlr, hrs, hrr, hfs, hfr,
+    ) = take(27)
 
     kv = lax.axis_index("kv")
     tp = lax.axis_index("tp")
@@ -80,7 +84,19 @@
     y = lax.rem(kv, NY)
     z = kv // NY
     yr, yl, yo = lax.rem(y + 1, NY), lax.rem(y + 3, NY), lax.rem(y + 2, NY)
-    right, left = z * NY + yr, z * NY + yl
+    right, left, opposite = z * NY + yr, z * NY + yl, z * NY + yo
+
+    def kv_peer(offset):
+        return lax.rem(z + offset[0], nz) * NY + lax.rem(y + offset[1], NY)
+
+    def tp_peer(offset):
+        return lax.rem(tp // 2 + offset[0], n_tp // 2) * 2 + lax.rem(lax.rem(tp, 2) + offset[1], 2)
+
+    barrier = pltpu.get_barrier_semaphore()
+    for o in pn.kv_far:
+        pl.semaphore_signal(barrier, inc=1, device_id={"kv": kv_peer(o)}, device_id_type=MESH)
+    for o in pn.tp_far:
+        pl.semaphore_signal(barrier, inc=1, device_id={"tp": tp_peer(o)}, device_id_type=MESH)
 
     pairs = [
         (tok_h, tok), (again_h, again), (wq_h, wq), (wk_h, wk), (wv_h, wv), (wg_h, wg),
@@ -99,16 +115,6 @@
     for c in loads:
         c.start()
 
-    barrier = pltpu.get_barrier_semaphore()
-
-    @pl.loop(1, n_kv)
-    def _(d):
-        pl.semaphore_signal(barrier, inc=1, device_id={"kv": lax.rem(kv + d, n_kv)}, device_id_type=MESH)
-
-    @pl.loop(1, n_tp)
-    def _(d):
-        pl.semaphore_signal(barrier, inc=1, device_id={"tp": lax.rem(tp + d, n_tp)}, device_id_type=MESH)
-
     def remote(src, dst, ssem, rsem, **where):
         return pltpu.make_async_remote_copy(
             src_ref=src, dst_ref=dst, send_sem=ssem, recv_sem=rsem, device_id=where, device_id_type=MESH
@@ -116,6 +122,8 @@
 
     def drain(ref, sem):
         pltpu.make_async_copy(ref, ref, sem).wait()
+
+    pending = []
 
     for c in loads[:7]:
         c.wait()
@@ -134,10 +142,10 @@
         p1[p] = f1[p * pn.seqs : (p + 1) * pn.seqs, :].astype(BF16)
     pl.semaphore_wait(barrier, n_kv + n_tp - 2)
 
-    @pl.loop(1, n_kv)
-    def _(d):
-        peer = lax.rem(kv + d, n_kv)
-        remote(p1.at[peer], r1.at[kv], s1s, s1r, kv=peer).start()
+    for o in pn.kv_far:
+        remote(p1.at[kv_peer(o)], r1.at[kv], s1s, s1r, kv=kv_peer(o)).start()
+
+    pending.append((p1.at[pl.ds(0, n_kv - 1)], s1s))
 
     r1[kv] = p1[kv]
 
@@ -203,10 +211,10 @@
     heads = normed * (out_gate / (1.0 + jnp.exp(-out_gate)))
     g1[kv] = heads.astype(BF16)
 
-    @pl.loop(1, n_kv)
-    def _(d):
-        peer = lax.rem(kv + d, n_kv)
-        remote(g1.at[kv], g1.at[kv], g1s, g1r, kv=peer).start()
+    for o in pn.kv_far:
+        remote(g1.at[kv], g1.at[kv], g1s, g1r, kv=kv_peer(o)).start()
+
+    pending.append((g1.at[pl.ds(0, n_kv - 1)], g1s))
 
     drain(g1.at[pl.ds(0, n_kv - 1)], g1r)
     for p in range(n_kv):
@@ -215,10 +223,10 @@
     def summed_over_tp(part, buf, ssem, rsem):
         buf[tp] = part.astype(BF16)
 
-        @pl.loop(1, n_tp)
-        def _(d):
-            peer = lax.rem(tp + d, n_tp)
-            remote(buf.at[tp], buf.at[tp], ssem, rsem, tp=peer).start()
+        for o in pn.tp_far:
+            remote(buf.at[tp], buf.at[tp], ssem, rsem, tp=tp_peer(o)).start()
+
+        pending.append((buf.at[pl.ds(0, n_tp - 1)], ssem))
 
         drain(buf.at[pl.ds(0, n_tp - 1)], rsem)
         total = buf[0].astype(F32)
@@ -231,16 +239,13 @@
     mid_f = mid.astype(F32)
     midt[...] = mid_f
     scaled_mid = (mid_f * mgt[...]).astype(BF16)
-    sq_rows = jnp.broadcast_to(jnp.sum(mid_f * mid_f, axis=0, keepdims=True), (UNIT, pn.rows)).astype(BF16)
+    sqb[kv] = jnp.sum(mid_f * mid_f, axis=0, keepdims=True)
 
     def fill(dest):
         gate = dot(gw[dest], scaled_mid).astype(BF16)
         up = dot(uw[dest], scaled_mid).astype(BF16)
         for s, zs in enumerate(pn.subs):
             at = 0
-            if pn.has_sq[s]:
-                psub[s][dest, 0:UNIT, :] = sq_rows
-                at = UNIT
             for zz in zs:
                 o, n = pn.off[zz], pn.cnt[zz]
                 psub[s][dest, at : at + n, :] = gate[o : o + n, :]
@@ -256,13 +261,19 @@
     fill(yo)
     for s in range(ns):
         remote(psub[s].at[yo], rin[s], rss.at[s], rsr.at[s], kv=toward(s)).start()
+        pending.append((rin[s], rss.at[s]))
     fill(yr)
     for s in range(pn.na, ns):
         remote(psub[s].at[yr], qin[s], qss.at[s], qsr.at[s], kv=right).start()
+        pending.append((qin[s], qss.at[s]))
     fill(yl)
     for s in range(pn.na):
         remote(psub[s].at[yl], qin[s], qss.at[s], qsr.at[s], kv=left).start()
+        pending.append((qin[s], qss.at[s]))
     fill(y)
+    for o in pn.kv_far:
+        remote(sqb.at[kv], sqb.at[kv], sqs, sqr, kv=kv_peer(o)).start()
+    pending.append((sqb.at[pl.ds(0, n_kv - 1)], sqs))
     order = []
     for i in range(max(pn.na, ns - pn.na)):
         order += [s for s in (i, pn.na + i) if (s < pn.na) == (s == i)]
@@ -271,39 +282,37 @@
         drain(rin[s], rsr.at[s])
         cout[s][...] = (psub[s][nxt].astype(F32) + rin[s][...].astype(F32)).astype(BF16)
         remote(cout[s], cin[s], css.at[s], csr.at[s], kv=toward(s)).start()
-    sq_sum = {}
+        pending.append((cin[s], css.at[s]))
     for s in order:
         drain(qin[s], qsr.at[s])
         drain(cin[s], csr.at[s])
         total = (psub[s][y].astype(F32) + qin[s][...].astype(F32) + cin[s][...].astype(F32)).astype(BF16)
-        side = s < pn.na
         at = 0
-        if pn.has_sq[s]:
-            sq_sum[side] = total[0:UNIT, :]
-            at = UNIT
         for zz in pn.subs[s]:
             n = pn.cnt[zz]
-            spc[zz, 0:UNIT, :] = sq_sum[side]
-            spc[zz, UNIT : UNIT + n, :] = total[at : at + n, :]
-            spc[zz, UNIT + pn.pr : UNIT + pn.pr + n, :] = total[at + n : at + 2 * n, :]
+            spc[zz, 0:n, :] = total[at : at + n, :]
+            spc[zz, pn.pr : pn.pr + n, :] = total[at + n : at + 2 * n, :]
             at += 2 * n
 
             @pl.when(z != zz)
             def _(zz=zz):
                 remote(spc.at[zz], zin.at[z], zss, zsr, kv=zz * NY + y).start()
 
+    pending.append((zin.at[pl.ds(0, nz - 1)], zss))
     zin[z] = spc[z]
     drain(zin.at[pl.ds(0, nz - 1)], zsr)
     total = zin[0].astype(F32)
     for i in range(1, nz):
         total = total + zin[i].astype(F32)
-    inv_mid = lax.rsqrt(total[0:1, :] / pn.width + EPS)
-    gate = total[UNIT : UNIT + pn.pr, :] * inv_mid
-    up = total[UNIT + pn.pr :, :] * inv_mid
+    drain(sqb.at[pl.ds(0, n_kv - 1)], sqr)
+    inv_mid = lax.rsqrt(jnp.sum(sqb[...], axis=0) / pn.width + EPS)
+    gate = total[0 : pn.pr, :] * inv_mid
+    up = total[pn.pr :, :] * inv_mid
     hb[y, z] = (gate / (1.0 + jnp.exp(-gate)) * up).astype(BF16)
 
-    for d in range(1, nz):
+    for d in sorted(range(1, nz), key=lambda d: -min(d, nz - d)):
         remote(hb.at[y, z], hb.at[y, z], hzs.at[d], hzr.at[d], kv=lax.rem(z + d, nz) * NY + y).start()
+        pending.append((hb.at[0, 0], hzs.at[d]))
 
     def slot(d):
         return lax.rem(z + nz - d, nz)
@@ -312,54 +321,39 @@
         if d:
             drain(hb.at[y, slot(d)], hzr.at[d])
         mine = hb.at[y, slot(d)]
+        remote(mine, mine, hfs.at[d], hfr.at[d], kv=opposite).start()
         remote(mine, mine, hls.at[d], hlr.at[d], kv=right).start()
         remote(mine, mine, hrs.at[d], hrr.at[d], kv=left).start()
-
-    def forward(d):
+        pending.append((hb.at[0, 0], hfs.at[d]))
+        pending.append((hb.at[0, 0], hls.at[d]))
+        pending.append((hb.at[0, 0], hrs.at[d]))
+
+    near = sorted(range(nz), key=lambda d: min(d, nz - d))
+    for d in near:
+        spread(d)
+
+    def lifted_from(row):
+        return dot(dnt[row], hb[row].reshape(nz * pn.pr, pn.rows))
+
+    lifted = lifted_from(y)
+    for d in near:
         drain(hb.at[yl, slot(d)], hlr.at[d])
         drain(hb.at[yr, slot(d)], hrr.at[d])
-        if d % 2 == 0:
-            other = hb.at[yl, slot(d)]
-            remote(other, other, hfs.at[d], hfr.at[d], kv=right).start()
-        else:
-            other = hb.at[yr, slot(d)]
-            remote(other, other, hfs.at[d], hfr.at[d], kv=left).start()
-
-    near = sorted(range(nz), key=lambda d: min(d, nz - d))
-    head, rest = near[:3], near[3:]
-    for d in head:
-        spread(d)
-    forward(near[0])
-    for d in rest:
-        spread(d)
-    for d in near[1:]:
-        forward(d)
-
-    def lifted_from(row):
-        return dot(dnt[row], hb[row].reshape(nz * pn.pr, pn.rows))
-
-    lifted = lifted_from(y) + lifted_from(yl) + lifted_from(yr)
+    lifted = lifted + lifted_from(yl) + lifted_from(yr)
     for d in near:
         drain(hb.at[yo, slot(d)], hfr.at[d])
     lifted = lifted + lifted_from(yo)
     final = midt[...] + summed_over_tp(lifted, x2, x2s, x2r)
     out_ref[...] = final.T.astype(BF16)
 
-    drain(p1.at[pl.ds(0, n_kv - 1)], s1s)
-    drain(g1.at[pl.ds(0, n_kv - 1)], g1s)
-    drain(x1.at[pl.ds(0, n_tp - 1)], x1s)
-    drain(x2.at[pl.ds(0, n_tp - 1)], x2s)
-    for s in range(ns):
-        drain(rin[s], rss.at[s])
-        drain(qin[s], qss.at[s])
-        drain(cin[s], css.at[s])
-    drain(zin.at[pl.ds(0, nz - 1)], zss)
-    for d in range(nz):
-        if d:
-            drain(hb.at[0, 0], hzs.at[d])
-        drain(hb.at[0, 0], hls.at[d])
-        drain(hb.at[0, 0], hrs.at[d])
-        drain(hb.at[0, 0], hfs.at[d])
+    for ref, sem in pending:
+        drain(ref, sem)
+
+
+def hand_over(a, b, c, ao, bo, co):
+    ao[...] = a[...]
+    bo[...] = b[...]
+    co[...] = c[...]
 
 
 def on_device(n_kv, n_tp, *args):
@@ -400,12 +394,13 @@
         vm((NY, nz * pr, feat), BF16), vm((NY, feat, nz * pr), BF16),
         vm((n_kv, seqs, vd), BF16), vm((rows, vd), F32), vm((n_tp, feat, rows), BF16),
         vm((feat, rows), F32), vm((n_tp, feat, rows), BF16),
-        vm((nz, pn.piece, rows), BF16), vm((nz, pn.piece, rows), BF16), vm((NY, nz, pr, rows), BF16),
+        vm((nz, 2 * pn.pr, rows), BF16), vm((nz, 2 * pn.pr, rows), BF16), vm((NY, nz, pr, rows), BF16),
+        vm((n_kv, 1, rows), F32),
     ]
     subs = [vm((NY, n, rows), BF16) for n in pn.sub_rows]
     for _ in range(4):
         subs += [vm((n, rows), BF16) for n in pn.sub_rows]
-    sems = [dma((17 + 3 * NY,))] + [dma(())] * 8 + [dma((ns,))] * 6 + [dma(())] * 2 + [dma((nz,))] * 8
+    sems = [dma((17 + 3 * NY,))] + [dma(())] * 10 + [dma((ns,))] * 6 + [dma(())] * 2 + [dma((nz,))] * 8
     out, nk, nv = pl.pallas_call(
         functools.partial(kernel, pn),
         out_shape=(
@@ -421,6 +416,17 @@
         ),
         name="decode_step",
     )(*operands)
+    out, nk, nv = pl.pallas_call(
+        hand_over,
+        out_shape=(
+            jax.ShapeDtypeStruct((rows, feat), BF16),
+            jax.ShapeDtypeStruct((seqs, kd), BF16),
+            jax.ShapeDtypeStruct((seqs, vd), BF16),
+        ),
+        in_specs=[pl.BlockSpec(memory_space=pltpu.VMEM)] * 3,
+        out_specs=(pl.BlockSpec(memory_space=pltpu.VMEM),) * 3,
+        name="hand_over",
+    )(out, nk, nv)
     return out, nk.reshape(seqs, 1, kd), nv.reshape(seqs, 1, vd)
 
 

time: 69.3 us -> 62.3 us (0.90)
  Pallas kernels: 65.8 us -> 61.4 us
  local copies, waits for them, and re-layouts: 2.62 us -> 0 us
    pallas_call x1, Pallas kernels: 65.8 us -> 60.1 us  [on_device(): pl.pallas_call(functools.partial(kernel, pn), out_shape=(jax.ShapeDtypeSt...]
    unnamed x7 -> x0, local copies, waits for them, and re-layouts: 2.62 us -> none
    pallas_call x0 -> x1, Pallas kernels: none -> 1.39 us  [on_device(): pl.pallas_call(hand_over, out_shape=(jax.ShapeDtypeStruct((rows, feat), B...]
where the time goes in v2:
time: 62.3 us; the launch traced here: 62.1 us
  Pallas kernels  61.4 us (99%)
  between operations  0.65 us (1%)
    pallas_call x1, Pallas kernels, on_device(): pl.pallas_call(functools.partial(kernel, pn), out_shape=(jax.ShapeDtypeSt...  60.1 us
    pallas_call x1, Pallas kernels, on_device(): pl.pallas_call(hand_over, out_shape=(jax.ShapeDtypeStruct((rows, feat), B...  1.39 us

profile of v2, /device:TPU:1, one launch (start us, length us, event | category | flops | bytes accessed | tf_op | source)
XLA Modules:
  0.0 62.1 jit_solution(15343908916116951527)
XLA Ops:
  0.6 60.1 %decode_step.1 = (bf16[128,128]{1,0:T(8,128)(2,1)}, bf16[4,128]{1,0:T(4,128)(2,1)}, bf16[4,256]{1,0:T(4,128)(2,1)}) custom-call(bf16[128,128]{1,0:T(8,128)(2,1)} %refs_0_.1, f32[1,128]{1,0:T(1,128)} %bitcast.21, bf16[128,128]{1,0:T(8,128)(2,1)} %refs_2_.1, bf16[128,128]{1,0:T(8,128)(2,1)} %refs_3_.1, bf16[128,256]{1,0:T(8,128)(2,1)} %refs_4_.1, ...), custom_call_target="tpu_custom_call" | custom-call | tf_op jit(solution)/shard_map/decode_step/pallas_call | solution.py:404
  60.7 1.4 %hand_over.1 = (bf16[128,128]{1,0:T(8,128)(2,1)}, bf16[4,128]{1,0:T(4,128)(2,1)}, bf16[4,256]{1,0:T(4,128)(2,1)}) custom-call(bf16[128,128]{1,0:T(8,128)(2,1)} %get-tuple-element.9.a, bf16[4,128]{1,0:T(4,128)(2,1)} %get-tuple-element.10.b, bf16[4,256]{1,0:T(4,128)(2,1)} %get-tuple-element.11.c), custom_call_target="tpu_custom_call" | custom-call | tf_op jit(solution)/shard_map/hand_over/pallas_call | solution.py:419
